TPU v7x, 32 devices: a whole 2x2x4 slice. The times are simulated.
32 devices in a mesh: grp: 2 (over y), sp: 4 (over z), tp: 4 (over x, core).
Axes of the slice: x: 2, y: 2, z: 4, core: 2. Of those that a mesh axis runs over, the one named last changes fastest.
Arguments:
- queries: bfloat16 [8192, 1024], P(('grp', 'sp'), 'tp'), parts along dimension 0, may hold values from -6 to 6
- keys: bfloat16 [8192, 256], P(('grp', 'sp')), parts along dimension 0, may hold values from -6 to 6
- values: bfloat16 [8192, 256], P(('grp', 'sp')), parts along dimension 0, may hold values from -6 to 6
- query_gain: float32 [128], replicated, may hold values from 1.2 to 6, as said below
- key_gain: float32 [128], replicated, may hold values from 1.2 to 6, as said below
- out_weight: bfloat16 [1024, 2048], replicated, may hold values from -6 to 6
- residual_in: bfloat16 [8192, 2048], P(('grp', 'sp', 'tp')), parts along dimension 0, may hold values from -6 to 6
- norm_gain: float32 [2048], replicated, may hold values from 0.1 to 1.9
- gate_weight: bfloat16 [2048, 2816], P('sp', 'tp'), may hold values from -0.125 to 0.125
- up_weight: bfloat16 [2048, 2816], P('sp', 'tp'), may hold values from -0.125 to 0.125
- down_weight: bfloat16 [2816, 2048], P('tp', 'sp'), may hold values from -0.109375 to 0.109375
Outputs:
- layer_out: bfloat16 [8192, 2048], P(('grp', 'sp', 'tp')), parts along dimension 0
There are 2 independent parts, one for each index of `grp`. A program takes and returns all parts, laid end to end along the dimension named above; an argument that names none is the same for every part. Nothing has to cross between parts.
Inputs may be any that keep to these rules, and one draw needn't show every extreme that they name: `query_gain`: positive gains. `key_gain`: positive gains.
All inputs are finite; a program needn't handle non-finite values.
Results may differ from a plain program's by a relative error of at most 0.015.
The roundings to bfloat16 on the way count: a program that leaves them out, or rounds other values in their place, can miss the bound.
Values may be sent and summed in bfloat16 or wider, within the bound.
A program may use at most 128 MiB of HBM per device.

v0:
```python
import jax
import jax.numpy as jnp
from jax import lax
from jax.sharding import PartitionSpec as P

HQ = 8
KV = 2
HD = 128
GRID_W = 64


def rotate(widened, positions):
    half = HD // 2
    inverse = 10000.0 ** (-jnp.arange(0, half, 2, dtype=jnp.float32) / half)
    grid_row = (positions // GRID_W).astype(jnp.float32)
    grid_col = (positions % GRID_W).astype(jnp.float32)
    angles = jnp.concatenate(
        [grid_row[:, None] * inverse[None], grid_col[:, None] * inverse[None]], axis=-1
    )
    cosine = jnp.cos(angles)[:, None, :]
    sine = jnp.sin(angles)[:, None, :]
    pairs = widened.reshape(widened.shape[0], widened.shape[1], half, 2)
    first = pairs[..., 0]
    second = pairs[..., 1]
    turned = jnp.stack([first * cosine - second * sine, first * sine + second * cosine], axis=-1)
    return turned.reshape(widened.shape)


def prepare(source, gain, positions, heads):
    widened = source.astype(jnp.float32).reshape(source.shape[0], heads, HD)
    widened = (
        widened * lax.rsqrt(jnp.mean(widened * widened, axis=-1, keepdims=True) + 1e-06) * gain
    )
    return rotate(widened, positions).astype(jnp.bfloat16)


def local(
    queries,
    keys,
    values,
    query_gain,
    key_gain,
    out_weight,
    residual_in,
    norm_gain,
    gate_weight,
    up_weight,
    down_weight,
):
    tok_rows = queries.shape[0]
    heads_here = queries.shape[1] // HD
    seq_index = lax.axis_index("sp")
    head_index = lax.axis_index("tp")
    positions = seq_index * tok_rows + jnp.arange(tok_rows, dtype=jnp.int32)
    query_rot = prepare(queries, query_gain, positions, heads_here)
    query_rot = query_rot.transpose(1, 0, 2).reshape(heads_here * tok_rows, HD)
    pair_index = head_index * heads_here // (HQ // KV)
    key_block = lax.dynamic_slice_in_dim(keys, pair_index * HD, HD, 1)
    value_block = lax.dynamic_slice_in_dim(values, pair_index * HD, HD, 1)
    key_rot = prepare(key_block, key_gain, positions, 1).reshape(tok_rows, HD)
    scale = HD ** (-0.5)

    def attend_block(carry, block):
        running_max, denominator, weighted = carry
        key_part, value_part = block
        scores = (
            lax.dot_general(
                query_rot, key_part, (((1,), (1,)), ((), ())), preferred_element_type=jnp.float32
            )
            * scale
        )
        new_max = jnp.maximum(running_max, jnp.max(scores, axis=1))
        factor = jnp.exp(running_max - new_max)
        raised = jnp.exp(scores - new_max[:, None])
        denominator = denominator * factor + jnp.sum(raised, axis=1)
        weighted = weighted * factor[:, None] + jnp.dot(
            raised.astype(jnp.bfloat16), value_part, preferred_element_type=jnp.float32
        )
        return ((new_max, denominator, weighted), None)

    start_carry = (
        jnp.full((heads_here * tok_rows,), -1e30, jnp.float32),
        jnp.zeros((heads_here * tok_rows,), jnp.float32),
        jnp.zeros((heads_here * tok_rows, HD), jnp.float32),
    )
    carry = start_carry
    pieces = (
        lax.all_gather(key_rot, "sp", axis=0, tiled=True),
        lax.all_gather(value_block, "sp", axis=0, tiled=True),
    )
    length = pieces[0].shape[0]
    block = tok_rows
    count = length // block
    key_parts = pieces[0].reshape(count, block, HD)
    value_parts = pieces[1].reshape(count, block, HD)
    carry, unused = lax.scan(attend_block, carry, (key_parts, value_parts))
    running_max, denominator, weighted = carry
    attended = (weighted / denominator[:, None]).astype(jnp.bfloat16)
    attended = (
        attended.reshape(heads_here, tok_rows, HD)
        .transpose(1, 0, 2)
        .reshape(tok_rows, heads_here * HD)
    )
    traded = lax.all_to_all(attended, "tp", split_axis=0, concat_axis=1, tiled=True)
    projected = jnp.dot(traded, out_weight, preferred_element_type=jnp.float32)
    middle = residual_in.astype(jnp.float32) + projected
    normed = (
        middle * lax.rsqrt(jnp.mean(middle * middle, axis=-1, keepdims=True) + 1e-06) * norm_gain
    )
    normed = normed.astype(jnp.bfloat16)
    rows_all = lax.all_gather(normed, "tp", axis=0, tiled=True)
    pieces = (
        lax.all_gather(gate_weight, "sp", axis=0, tiled=True),
        lax.all_gather(up_weight, "sp", axis=0, tiled=True),
    )
    gate_act = jnp.dot(rows_all, pieces[0], preferred_element_type=jnp.float32)
    up_act = jnp.dot(rows_all, pieces[1], preferred_element_type=jnp.float32)
    down_all = lax.all_gather(down_weight, "sp", axis=1, tiled=True)
    hidden = (jax.nn.silu(gate_act) * up_act).astype(jnp.bfloat16)
    mixer_out = lax.psum_scatter(
        jnp.dot(hidden, down_all, preferred_element_type=jnp.float32).astype(jnp.bfloat16),
        "tp",
        scatter_dimension=0,
        tiled=True,
    ).astype(jnp.float32)
    return (middle + mixer_out).astype(jnp.bfloat16)


def solution(mesh):
    placed = (
        P(("grp", "sp"), "tp"),
        P(("grp", "sp"), None),
        P(("grp", "sp"), None),
        P(),
        P(),
        P(),
        P(("grp", "sp", "tp"), None),
        P(),
        P("sp", "tp"),
        P("sp", "tp"),
        P("tp", "sp"),
    )
    return jax.shard_map(
        local, mesh=mesh, in_specs=placed, out_specs=P(("grp", "sp", "tp"), None), check_vma=False
    )
```

profile of v0, /device:TPU:0, one launch (start us, length us, event | category | flops | bytes accessed | tf_op | source)
XLA Modules:
  0.0 361.1 jit_solution(3886411990185898844)
XLA Ops:
  6.6 1.2 fusion.18
  7.8 1.2 fusion.19
  10.1 1.0 subtract_convert_fusion.1
  11.4 0.8 convert_element_type.62
  12.3 0.7 constant_dynamic-slice_fusion
  13.1 0.7 all-gather.13.cloned.1.call-update
  13.9 1.0 convert_multiply_fusion.2
  15.2 2.7 mul.248
  17.9 2.4 reduce_sum.37
  20.5 1.6 reshape.340
  22.3 1.1 fusion.21
  23.4 1.7 multiply_multiply_fusion
  25.1 1.4 subtract_convert_fusion
  26.5 1.2 pad_maximum_fusion
  27.7 0.5 copy.37
  28.3 0.5 copy.43
  28.8 14.3 %all-gather.7.cloned.1.call-done = bf16[4096,128]{0,1:T(8,128)(2,1)} async-done(((bf16[1024,128]{0,1:T(8,128)(2,1)}), bf16[4096,128]{0,1:T(8,128)(2,1)}) %all-gather.7.cloned.1.call-update) | async-done | bytes 1048592 | tf_op jit(solution)/shard_map/all_gather | solution.py:88
  43.1 1.6 copy.42
  44.7 27.3 %all-gather.9.cloned.1.call-done = bf16[4096,128]{1,0:T(8,128)(2,1)} async-done(((bf16[1024,128]{1,0:T(8,128)(2,1)}), bf16[4096,128]{1,0:T(8,128)(2,1)}) %all-gather.9.cloned.1.call-update) | async-done | bytes 1048592 | tf_op jit(solution)/shard_map/all_gather | solution.py:89
  72.1 53.6 %while.15 = (s32[]{:T(128)}, f32[2048]{0:T(1024)S(1)}, f32[2048]{0:T(1024)S(1)}, f32[2048,128]{1,0:T(8,128)S(1)}, bf16[4,1024,128]{2,1,0:T(8,128)(2,1)S(1)}, /*i...) while((s32[]{:T(128)}, f32[2048]{0:T(1024)S(1)}, ...), condition=%wide.region_5.6_spmd.clone, body=%wide.region_2.5_spmd.clone.sunk | while | flops 1091315712 | bytes 61997704 | solution.py:96
  72.1 4.5 %multiply_reduce_fusion.3 = (f32[2048]{0:T(1024)S(1)}, f32[1024,2048]{1,0:T(8,128)}) fusion(bf16[2048,128]{1,0:T(8,128)(2,1)S(1)} %get-tuple-element.200, bf16[4,1024,128]{2,1,0:T(8,128)(2,1)S(1)} %get-tuple-element.199, s32[]{:T(128)} %get-tuple-element.186), kind=kOutput, calls=%fused_computation.1.clone.1 | convolution fusion | flops 541063168 | bytes 9183236 | tf_op jit(solution)/shard_map/while/body/eval_jaxpr/dot_general | solution.py:67
  76.6 5.1 %fusion.53 = f32[2048]{0:T(1024)S(1)} fusion(f32[1024,2048]{1,0:T(8,128)} %get-tuple-element.174, f32[2048]{0:T(1024)S(1)} %select_maximum_fusion.2), kind=kLoop, calls=%fused_computation.3.clone.1 | loop fusion | flops 6289408 | bytes 8404992 | tf_op jit(solution)/shard_map/while/body/eval_jaxpr/reduce_sum | solution.py:75
  81.7 1.3 copy-done.1
  83.0 2.9 fusion.55
  86.0 4.5 %multiply_reduce_fusion.3 = (f32[2048]{0:T(1024)S(1)}, f32[1024,2048]{1,0:T(8,128)}) fusion(bf16[2048,128]{1,0:T(8,128)(2,1)S(1)} %get-tuple-element.200, bf16[4,1024,128]{2,1,0:T(8,128)(2,1)S(1)} %get-tuple-element.199, s32[]{:T(128)} %get-tuple-element.186), kind=kOutput, calls=%fused_computation.1.clone.1 | convolution fusion | flops 541063168 | bytes 9183236 | tf_op jit(solution)/shard_map/while/body/eval_jaxpr/dot_general | solution.py:67
  90.5 5.0 %fusion.53 = f32[2048]{0:T(1024)S(1)} fusion(f32[1024,2048]{1,0:T(8,128)} %get-tuple-element.174, f32[2048]{0:T(1024)S(1)} %select_maximum_fusion.2), kind=kLoop, calls=%fused_computation.3.clone.1 | loop fusion | flops 6289408 | bytes 8404992 | tf_op jit(solution)/shard_map/while/body/eval_jaxpr/reduce_sum | solution.py:75
  95.4 0.9 copy-done.1
  96.3 2.9 fusion.55
  99.2 4.5 %multiply_reduce_fusion.3 = (f32[2048]{0:T(1024)S(1)}, f32[1024,2048]{1,0:T(8,128)}) fusion(bf16[2048,128]{1,0:T(8,128)(2,1)S(1)} %get-tuple-element.200, bf16[4,1024,128]{2,1,0:T(8,128)(2,1)S(1)} %get-tuple-element.199, s32[]{:T(128)} %get-tuple-element.186), kind=kOutput, calls=%fused_computation.1.clone.1 | convolution fusion | flops 541063168 | bytes 9183236 | tf_op jit(solution)/shard_map/while/body/eval_jaxpr/dot_general | solution.py:67
  103.7 5.0 %fusion.53 = f32[2048]{0:T(1024)S(1)} fusion(f32[1024,2048]{1,0:T(8,128)} %get-tuple-element.174, f32[2048]{0:T(1024)S(1)} %select_maximum_fusion.2), kind=kLoop, calls=%fused_computation.3.clone.1 | loop fusion | flops 6289408 | bytes 8404992 | tf_op jit(solution)/shard_map/while/body/eval_jaxpr/reduce_sum | solution.py:75
  108.7 0.8 copy-done.1
  109.6 2.9 fusion.55
  112.5 4.5 %multiply_reduce_fusion.3 = (f32[2048]{0:T(1024)S(1)}, f32[1024,2048]{1,0:T(8,128)}) fusion(bf16[2048,128]{1,0:T(8,128)(2,1)S(1)} %get-tuple-element.200, bf16[4,1024,128]{2,1,0:T(8,128)(2,1)S(1)} %get-tuple-element.199, s32[]{:T(128)} %get-tuple-element.186), kind=kOutput, calls=%fused_computation.1.clone.1 | convolution fusion | flops 541063168 | bytes 9183236 | tf_op jit(solution)/shard_map/while/body/eval_jaxpr/dot_general | solution.py:67
  117.0 5.0 %fusion.53 = f32[2048]{0:T(1024)S(1)} fusion(f32[1024,2048]{1,0:T(8,128)} %get-tuple-element.174, f32[2048]{0:T(1024)S(1)} %select_maximum_fusion.2), kind=kLoop, calls=%fused_computation.3.clone.1 | loop fusion | flops 6289408 | bytes 8404992 | tf_op jit(solution)/shard_map/while/body/eval_jaxpr/reduce_sum | solution.py:75
  122.0 0.8 copy-done.1
  122.8 2.9 fusion.55
  126.1 0.5 copy.51
  126.9 11.2 %all_to_all.19 = bf16[4,256,256]{2,1,0:T(8,128)(2,1)S(1)} all-to-all(bf16[4,256,256]{2,1,0:T(8,128)(2,1)S(1)} %all_to_all.14), channel_id=1, replica_groups=mesh['grp'=2,'sp'=4,'tp'=4] {'tp'}, dimensions={0} | all-to-all | bytes 1048576 | tf_op jit(solution)/shard_map/all_to_all | solution.py:104
  138.4 3.9 %multiply_reduce_fusion.1 = (f32[256]{0:T(256)S(1)}, f32[256,2048]{1,0:T(8,128)S(1)}) fusion(bf16[256,1024]{0,1:T(8,128)(2,1)S(1)} %bitcast.46, bf16[1024,2048]{1,0:T(8,128)(2,1)} %param.18, bf16[256,2048]{1,0:T(8,128)(2,1)} %param.19), kind=kOutput, calls=%fused_computation.26 | convolution fusion | flops 1075838720 | bytes 7865344 | tf_op jit(solution)/shard_map/dot_general | solution.py:105
  142.3 1.2 multiply_convert_fusion.1
  143.6 0.5 all-gather.15.cloned.1.call-update
  145.0 31.5 %all-gather.11.cloned.1.call-done = bf16[1024,2048]{1,0:T(8,128)(2,1)} async-done(((bf16[256,2048]{1,0:T(8,128)(2,1)}), bf16[1024,2048]{1,0:T(8,128)(2,1)}) %all-gather.11.cloned.1.call-update) | async-done | bytes 4194320 | tf_op jit(solution)/shard_map/all_gather | solution.py:111
  176.5 7.8 %fusion.35 = f32[1024,704]{0,1:T(8,128)} fusion(bf16[1024,2048]{1,0:T(8,128)(2,1)} %all-gather.11.cloned.1.call-done, bf16[2048,704]{0,1:T(8,128)(2,1)} %all-gather.13.cloned.1.call-done), kind=kOutput, calls=%fused_computation.72 | convolution fusion | flops 2952790016 | bytes 9961472 | tf_op jit(solution)/shard_map/dot_general | solution.py:116
  184.3 52.7 %all-gather.15.cloned.1.call-done = bf16[2048,704]{0,1:T(8,128)(2,1)} async-done(((bf16[512,704]{0,1:T(8,128)(2,1)}), bf16[2048,704]{0,1:T(8,128)(2,1)}) %all-gather.15.cloned.1.call-update) | async-done | bytes 2883600 | tf_op jit(solution)/shard_map/all_gather | solution.py:114
  237.1 59.3 %all-gather.17.cloned.1.call-done = bf16[704,2048]{1,0:T(8,128)(2,1)} async-done(((bf16[704,512]{1,0:T(8,128)(2,1)}), bf16[704,2048]{1,0:T(8,128)(2,1)}) %all-gather.17.cloned.1.call-update) | async-done | bytes 2883600 | tf_op jit(solution)/shard_map/all_gather | solution.py:118
  296.3 12.0 %convolution_convert_fusion = bf16[1024,2048]{1,0:T(8,128)(2,1)} fusion(bf16[704,2048]{1,0:T(8,128)(2,1)} %all-gather.17.cloned.1.call-done, f32[1024,704]{0,1:T(8,128)} %fusion.35, bf16[1024,2048]{1,0:T(8,128)(2,1)} %all-gather.11.cloned.1.call-done, bf16[2048,704]{0,1:T(8,128)(2,1)} %all-gather.15.cloned.1.call-done), kind=kOutput, calls=%fused_computation.21 | convolution fusion | flops 5912002560 | bytes 17039360 | tf_op jit(solution)/shard_map/dot_general | solution.py:121
  308.4 43.4 %reduce-scatter.2.cloned.1.call-done = bf16[256,2048]{1,0:T(8,128)(2,1)} async-done(((bf16[1024,2048]{1,0:T(8,128)(2,1)}), bf16[256,2048]{1,0:T(8,128)(2,1)}) %reduce-scatter.2.cloned.1.call-update) | async-done | bytes 1048592 | tf_op jit(solution)/shard_map/reduce_scatter | solution.py:120
  351.8 2.5 add_convert_fusion
  (57 shorter events, 3.9 us)
Async XLA Ops:
  6.5 5.8 %copy-start = (bf16[1024,256]{1,0:T(8,128)(2,1)S(1)}, bf16[1024,256]{1,0:T(8,128)(2,1)}, u32[]{:S(2)}) copy-start(bf16[1024,256]{1,0:T(8,128)(2,1)} %param.15) | copy-start | bytes 1572868
  6.5 36.6 %all-gather.7.cloned.1.call-start = ((), (), s32[]{:S(2)}) async-start(), calls=%async_computation.2 | async-start | bytes 1310720 | tf_op jit(solution)/shard_map/all_gather | solution.py:88
  9.5 4.4 %copy-start.2 = (bf16[1024,256]{1,0:T(8,128)(2,1)S(1)}, bf16[1024,256]{1,0:T(8,128)(2,1)}, u32[]{:S(2)}) copy-start(bf16[1024,256]{1,0:T(8,128)(2,1)} %param.13) | copy-start | bytes 1572868
  12.3 59.8 %all-gather.9.cloned.1.call-start = ((), (), s32[]{:S(2)}) async-start(), calls=%async_computation.3 | async-start | bytes 1310720 | tf_op jit(solution)/shard_map/all_gather | solution.py:89
  13.1 131.9 %all-gather.13.cloned.1.call-start = ((), (), s32[]{:S(2)}) async-start(), calls=%async_computation.5 | async-start | bytes 3604480 | tf_op jit(solution)/shard_map/all_gather | solution.py:113
  13.8 162.7 %all-gather.11.cloned.1.call-start = ((), (), s32[]{:S(2)}) async-start(), calls=%async_computation.4 | async-start | bytes 5242880 | tf_op jit(solution)/shard_map/all_gather | solution.py:111
  15.2 7.0 %copy-start.4 = (f32[128]{0:T(128)S(1)}, f32[128]{0:T(128)}, u32[]{:S(2)}) copy-start(f32[128]{0:T(128)} %param.16) | copy-start | bytes 1540
  76.6 6.5 %copy-start.1 = (f32[1024,2048]{1,0:T(8,128)S(1)}, f32[1024,2048]{1,0:T(8,128)}, u32[]{:S(2)}) copy-start(f32[1024,2048]{1,0:T(8,128)} %get-tuple-element.174) | copy-start | bytes 25165828 | tf_op jit(solution)/shard_map/while
  90.5 5.9 %copy-start.1 = (f32[1024,2048]{1,0:T(8,128)S(1)}, f32[1024,2048]{1,0:T(8,128)}, u32[]{:S(2)}) copy-start(f32[1024,2048]{1,0:T(8,128)} %get-tuple-element.174) | copy-start | bytes 25165828 | tf_op jit(solution)/shard_map/while
  103.7 5.8 %copy-start.1 = (f32[1024,2048]{1,0:T(8,128)S(1)}, f32[1024,2048]{1,0:T(8,128)}, u32[]{:S(2)}) copy-start(f32[1024,2048]{1,0:T(8,128)} %get-tuple-element.174) | copy-start | bytes 25165828 | tf_op jit(solution)/shard_map/while
  117.0 5.8 %copy-start.1 = (f32[1024,2048]{1,0:T(8,128)S(1)}, f32[1024,2048]{1,0:T(8,128)}, u32[]{:S(2)}) copy-start(f32[1024,2048]{1,0:T(8,128)} %get-tuple-element.174) | copy-start | bytes 25165828 | tf_op jit(solution)/shard_map/while
  138.4 3.9 %copy-start.3 = (f32[2048]{0:T(1024)S(1)}, f32[2048]{0:T(1024)}, u32[]{:S(2)}) copy-start(f32[2048]{0:T(1024)} %param.20) | copy-start | bytes 24580
  143.5 93.5 %all-gather.15.cloned.1.call-start = ((), (), s32[]{:S(2)}) async-start(), calls=%async_computation.6 | async-start | bytes 3604480 | tf_op jit(solution)/shard_map/all_gather | solution.py:114
  144.1 152.2 %all-gather.17.cloned.1.call-start = ((), (), s32[]{:S(2)}) async-start(), calls=%async_computation.7 | async-start | bytes 3604480 | tf_op jit(solution)/shard_map/all_gather | solution.py:118
  144.7 207.1 %reduce-scatter.2.cloned.1.call-start = ((), (), s32[]{:S(2)}) async-start(), calls=%async_computation.8 | async-start | bytes 5242880 | tf_op jit(solution)/shard_map/reduce_scatter | solution.py:120
Sparse Core Ops, SparseCore 0:
  12.4 30.6 all-gather.6
  44.7 27.3 all-gather.8
  73.7 58.4 all-gather.12
  143.6 32.8 all-gather.10
  177.9 59.1 all-gather.14
  238.5 57.7 all-gather.16
  308.5 43.2 reduce-scatter.1
where the time goes:
time: 362 us; the launch traced here: 361 us
  waiting for transfers between devices  230 us (64%)
  matrix products  53.2 us (15%)
  other arithmetic  36.6 us (10%)
  local copies, waits for them, and re-layouts  15.3 us (4%)
  between operations  13.8 us (4%)
  blocking collectives  11.2 us (3%)
    all_gather x1, waiting for transfers between devices, local(): down_all = lax.all_gather(down_weight, 'sp', axis=1, tiled=True)  59.3 us
    all_gather x1, waiting for transfers between devices, local(): lax.all_gather(up_weight, 'sp', axis=0, tiled=True)  52.7 us
    reduce_scatter x1, waiting for transfers between devices, local(): lax.psum_scatter(jnp.dot(hidden, down_all, preferred_element_type=jnp.flo...  43.4 us
    all_gather x1, waiting for transfers between devices, local(): rows_all = lax.all_gather(normed, 'tp', axis=0, tiled=True)  31.5 us
    all_gather x1, waiting for transfers between devices, local(): lax.all_gather(value_block, 'sp', axis=0, tiled=True)  27.3 us
    reduce_sum x4, other arithmetic, attend_block(): denominator = denominator * factor + jnp.sum(raised, axis=1)  20 us
    dot_general x4, matrix products, attend_block(): lax.dot_general(query_rot, key_part, (((1,), (1,)), ((), ())), preferred_...  18 us
    all_gather x1, waiting for transfers between devices, local(): lax.all_gather(key_rot, 'sp', axis=0, tiled=True)  14.3 us
  transfers between devices with their start and end apart: 7, of which 6 were waited for; matrix products, arithmetic and copies ran while one was open for 22% of the time, Pallas kernels for 0%

commit v1 on v0

--- a/solution.py
+++ b/solution.py
@@ -7,6 +7,17 @@
 KV = 2
 HD = 128
 GRID_W = 64
+
+
+def gather_by_hops(value, axis, d):
+    devices = lax.axis_size(axis)
+    right = [(i, (i + 1) % devices) for i in range(devices)]
+    parts = [value]
+    for far in range(1, devices):
+        parts = [lax.ppermute(parts[0], axis, right), *parts]
+    whole = jnp.concatenate(parts, axis=d)
+    turn = (lax.axis_index(axis) + 1) * parts[-1].shape[d]
+    return jnp.roll(whole, turn, axis=d)
 
 
 def rotate(widened, positions):
@@ -108,7 +119,7 @@
         middle * lax.rsqrt(jnp.mean(middle * middle, axis=-1, keepdims=True) + 1e-06) * norm_gain
     )
     normed = normed.astype(jnp.bfloat16)
-    rows_all = lax.all_gather(normed, "tp", axis=0, tiled=True)
+    rows_all = gather_by_hops(normed, "tp", 0)
     pieces = (
         lax.all_gather(gate_weight, "sp", axis=0, tiled=True),
         lax.all_gather(up_weight, "sp", axis=0, tiled=True),

time: 362 us -> 316 us (0.87)
  waiting for transfers between devices: 230 us -> 169 us
  local copies, waits for them, and re-layouts: 15.3 us -> 29.2 us
    all_gather x1, waiting for transfers between devices: 52.7 us -> 0.01 us  [local(): lax.all_gather(up_weight, 'sp', axis=0, tiled=True)]
    ppermute x0 -> x3, waiting for transfers between devices: none -> 43.3 us  [gather_by_hops(): parts = [lax.ppermute(parts[0], axis, right), *parts]]
    all_gather x1 -> x0, waiting for transfers between devices: 31.5 us -> none  [local(): rows_all = lax.all_gather(normed, 'tp', axis=0, tiled=True)]
    all_gather x1, waiting for transfers between devices: 59.3 us -> 40 us  [local(): down_all = lax.all_gather(down_weight, 'sp', axis=1, tiled=True)]
    unnamed x10 -> x18, local copies, waits for them, and re-layouts: 2.17 us -> 16.1 us
  transfers between devices with their start and end apart: 7 -> 9, of which waited for: 6 -> 7; matrix products, arithmetic and copies ran while one was open for 22% -> 31% of each run, Pallas kernels for 0% -> 0%
where the time goes in v1:
time: 316 us
  waiting for transfers between devices  169 us (53%)
  matrix products  53.7 us (17%)
  other arithmetic  38.1 us (12%)
  local copies, waits for them, and re-layouts  29.2 us (9%)
  between operations  13.8 us (4%)
  blocking collectives  11.2 us (4%)
    reduce_scatter x1, waiting for transfers between devices, local(): lax.psum_scatter(jnp.dot(hidden, down_all, preferred_element_type=jnp.flo...  43.4 us
    ppermute x3, waiting for transfers between devices, gather_by_hops(): parts = [lax.ppermute(parts[0], axis, right), *parts]  43.3 us
    all_gather x1, waiting for transfers between devices, local(): down_all = lax.all_gather(down_weight, 'sp', axis=1, tiled=True)  40 us
    all_gather x1, waiting for transfers between devices, local(): lax.all_gather(value_block, 'sp', axis=0, tiled=True)  27.3 us
    reduce_sum x4, other arithmetic, attend_block(): denominator = denominator * factor + jnp.sum(raised, axis=1)  20 us
    dot_general x4, matrix products, attend_block(): lax.dot_general(query_rot, key_part, (((1,), (1,)), ((), ())), preferred_...  18 us
    unnamed x18, local copies, waits for them, and re-layouts  16.1 us
    all_gather x1, waiting for transfers between devices, local(): lax.all_gather(key_rot, 'sp', axis=0, tiled=True)  13.8 us
  transfers between devices with their start and end apart: 9, of which 7 were waited for; matrix products, arithmetic and copies ran while one was open for 31% of the time, Pallas kernels for 0%

profile of v1, /device:TPU:0, one launch (start us, length us, event | category | flops | bytes accessed | tf_op | source)
XLA Modules:
  0.0 315.6 jit_solution(2938891268032677530)
XLA Ops:
  6.6 1.2 fusion.27
  7.8 1.2 fusion.28
  10.1 1.0 subtract_convert_fusion.1
  14.4 1.0 convert_multiply_fusion.2
  15.7 2.7 mul.251
  18.5 2.4 reduce_sum.37
  21.1 1.6 reshape.340
  22.8 1.1 fusion.30
  24.0 1.7 multiply_multiply_fusion
  25.6 1.4 subtract_convert_fusion
  27.1 1.2 pad_maximum_fusion
  29.4 13.8 %all-gather.6.cloned.1.call-done = bf16[4096,128]{0,1:T(8,128)(2,1)} async-done(((bf16[1024,128]{0,1:T(8,128)(2,1)}), bf16[4096,128]{0,1:T(8,128)(2,1)}) %all-gather.6.cloned.1.call-update) | async-done | bytes 1048592 | tf_op jit(solution)/shard_map/all_gather | solution.py:99
  43.1 1.6 copy.42
  44.7 27.3 %all-gather.8.cloned.1.call-done = bf16[4096,128]{1,0:T(8,128)(2,1)} async-done(((bf16[1024,128]{1,0:T(8,128)(2,1)}), bf16[4096,128]{1,0:T(8,128)(2,1)}) %all-gather.8.cloned.1.call-update) | async-done | bytes 1048592 | tf_op jit(solution)/shard_map/all_gather | solution.py:100
  72.1 53.6 %while.15 = (s32[]{:T(128)}, f32[2048]{0:T(1024)S(1)}, f32[2048]{0:T(1024)S(1)}, f32[2048,128]{1,0:T(8,128)S(1)}, bf16[4,1024,128]{2,1,0:T(8,128)(2,1)S(1)}, /*i...) while((s32[]{:T(128)}, f32[2048]{0:T(1024)S(1)}, ...), condition=%wide.region_5.6_spmd.clone, body=%wide.region_2.5_spmd.clone.sunk | while | flops 1091315712 | bytes 61997704 | solution.py:107
  72.1 4.5 %multiply_reduce_fusion.3 = (f32[2048]{0:T(1024)S(1)}, f32[1024,2048]{1,0:T(8,128)}) fusion(bf16[2048,128]{1,0:T(8,128)(2,1)S(1)} %get-tuple-element.200, bf16[4,1024,128]{2,1,0:T(8,128)(2,1)S(1)} %get-tuple-element.199, s32[]{:T(128)} %get-tuple-element.186), kind=kOutput, calls=%fused_computation.1.clone.1 | convolution fusion | flops 541063168 | bytes 9183236 | tf_op jit(solution)/shard_map/while/body/eval_jaxpr/dot_general | solution.py:78
  76.6 5.1 %fusion.62 = f32[2048]{0:T(1024)S(1)} fusion(f32[1024,2048]{1,0:T(8,128)} %get-tuple-element.174, f32[2048]{0:T(1024)S(1)} %select_maximum_fusion.2), kind=kLoop, calls=%fused_computation.3.clone.1 | loop fusion | flops 6289408 | bytes 8404992 | tf_op jit(solution)/shard_map/while/body/eval_jaxpr/reduce_sum | solution.py:86
  81.7 1.3 copy-done.2
  83.0 2.9 fusion.64
  86.0 4.5 %multiply_reduce_fusion.3 = (f32[2048]{0:T(1024)S(1)}, f32[1024,2048]{1,0:T(8,128)}) fusion(bf16[2048,128]{1,0:T(8,128)(2,1)S(1)} %get-tuple-element.200, bf16[4,1024,128]{2,1,0:T(8,128)(2,1)S(1)} %get-tuple-element.199, s32[]{:T(128)} %get-tuple-element.186), kind=kOutput, calls=%fused_computation.1.clone.1 | convolution fusion | flops 541063168 | bytes 9183236 | tf_op jit(solution)/shard_map/while/body/eval_jaxpr/dot_general | solution.py:78
  90.5 5.0 %fusion.62 = f32[2048]{0:T(1024)S(1)} fusion(f32[1024,2048]{1,0:T(8,128)} %get-tuple-element.174, f32[2048]{0:T(1024)S(1)} %select_maximum_fusion.2), kind=kLoop, calls=%fused_computation.3.clone.1 | loop fusion | flops 6289408 | bytes 8404992 | tf_op jit(solution)/shard_map/while/body/eval_jaxpr/reduce_sum | solution.py:86
  95.4 0.9 copy-done.2
  96.3 2.9 fusion.64
  99.2 4.5 %multiply_reduce_fusion.3 = (f32[2048]{0:T(1024)S(1)}, f32[1024,2048]{1,0:T(8,128)}) fusion(bf16[2048,128]{1,0:T(8,128)(2,1)S(1)} %get-tuple-element.200, bf16[4,1024,128]{2,1,0:T(8,128)(2,1)S(1)} %get-tuple-element.199, s32[]{:T(128)} %get-tuple-element.186), kind=kOutput, calls=%fused_computation.1.clone.1 | convolution fusion | flops 541063168 | bytes 9183236 | tf_op jit(solution)/shard_map/while/body/eval_jaxpr/dot_general | solution.py:78
  103.7 5.0 %fusion.62 = f32[2048]{0:T(1024)S(1)} fusion(f32[1024,2048]{1,0:T(8,128)} %get-tuple-element.174, f32[2048]{0:T(1024)S(1)} %select_maximum_fusion.2), kind=kLoop, calls=%fused_computation.3.clone.1 | loop fusion | flops 6289408 | bytes 8404992 | tf_op jit(solution)/shard_map/while/body/eval_jaxpr/reduce_sum | solution.py:86
  108.7 0.8 copy-done.2
  109.6 2.9 fusion.64
  112.5 4.5 %multiply_reduce_fusion.3 = (f32[2048]{0:T(1024)S(1)}, f32[1024,2048]{1,0:T(8,128)}) fusion(bf16[2048,128]{1,0:T(8,128)(2,1)S(1)} %get-tuple-element.200, bf16[4,1024,128]{2,1,0:T(8,128)(2,1)S(1)} %get-tuple-element.199, s32[]{:T(128)} %get-tuple-element.186), kind=kOutput, calls=%fused_computation.1.clone.1 | convolution fusion | flops 541063168 | bytes 9183236 | tf_op jit(solution)/shard_map/while/body/eval_jaxpr/dot_general | solution.py:78
  117.0 5.0 %fusion.62 = f32[2048]{0:T(1024)S(1)} fusion(f32[1024,2048]{1,0:T(8,128)} %get-tuple-element.174, f32[2048]{0:T(1024)S(1)} %select_maximum_fusion.2), kind=kLoop, calls=%fused_computation.3.clone.1 | loop fusion | flops 6289408 | bytes 8404992 | tf_op jit(solution)/shard_map/while/body/eval_jaxpr/reduce_sum | solution.py:86
  122.8 2.9 fusion.64
  126.9 11.2 %all_to_all.19 = bf16[4,256,256]{2,1,0:T(8,128)(2,1)S(1)} all-to-all(bf16[4,256,256]{2,1,0:T(8,128)(2,1)S(1)} %all_to_all.14), channel_id=1, replica_groups=mesh['grp'=2,'sp'=4,'tp'=4] {'tp'}, dimensions={0} | all-to-all | bytes 1048576 | tf_op jit(solution)/shard_map/all_to_all | solution.py:115
  138.4 4.2 %multiply_reduce_fusion.1 = (f32[256]{0:T(256)S(1)}, f32[256,2048]{1,0:T(8,128)S(1)}) fusion(bf16[256,1024]{0,1:T(8,128)(2,1)S(1)} %bitcast.44, bf16[1024,2048]{1,0:T(8,128)(2,1)} %param.18, bf16[256,2048]{1,0:T(8,128)(2,1)} %param.19), kind=kOutput, calls=%fused_computation.30 | convolution fusion | flops 1075838720 | bytes 7865344 | tf_op jit(solution)/shard_map/dot_general | solution.py:116
  142.9 14.3 %collective-permute-done = bf16[256,2048]{1,0:T(8,128)(2,1)} collective-permute-done((bf16[256,2048]{1,0:T(8,128)(2,1)S(1)}, bf16[256,2048]{1,0:T(8,128)(2,1)}, u32[]{:S(2)}, u32[]{:S(2)}) %collective-permute-start) | collective-permute-done | bytes 1048608 | tf_op jit(solution)/shard_map/ppermute | solution.py:17
  157.3 14.5 %collective-permute-done.1 = bf16[256,2048]{1,0:T(8,128)(2,1)} collective-permute-done((bf16[256,2048]{1,0:T(8,128)(2,1)}, bf16[256,2048]{1,0:T(8,128)(2,1)}, u32[]{:S(2)}, u32[]{:S(2)}) %collective-permute-start.1) | collective-permute-done | bytes 1048608 | tf_op jit(solution)/shard_map/ppermute | solution.py:17
  171.8 14.5 %collective-permute-done.2 = bf16[256,2048]{1,0:T(8,128)(2,1)} collective-permute-done((bf16[256,2048]{1,0:T(8,128)(2,1)}, bf16[256,2048]{1,0:T(8,128)(2,1)}, u32[]{:S(2)}, u32[]{:S(2)}) %collective-permute-start.2) | collective-permute-done | bytes 1048608 | tf_op jit(solution)/shard_map/ppermute | solution.py:17
  186.3 2.3 constant_dynamic-update-slice_fusion.7
  188.7 2.3 constant_dynamic-update-slice_fusion.6
  191.0 2.3 constant_dynamic-update-slice_fusion.5
  193.3 1.2 constant_dynamic-update-slice_fusion.4
  194.5 2.3 constant_dynamic-update-slice_fusion.3
  196.8 2.4 constant_dynamic-update-slice_fusion.2
  199.2 2.4 constant_dynamic-update-slice_fusion.1
  201.5 1.3 constant_dynamic-update-slice_fusion
  202.8 7.8 %fusion.18 = f32[1024,704]{0,1:T(8,128)} fusion(bf16[2048,704]{0,1:T(8,128)(2,1)} %all-gather.12.cloned.1.call-done, bf16[2048,2048]{1,0:T(8,128)(2,1)} %constant_dynamic-update-slice_fusion, s32[]{:T(128)S(6)} %select_n.48), kind=kOutput, calls=%fused_computation.22 | convolution fusion | flops 2952790016 | bytes 9961476 | tf_op jit(solution)/shard_map/dot_general | solution.py:128
  210.7 40.0 %all-gather.14.cloned.1.call-done = bf16[704,2048]{1,0:T(8,128)(2,1)} async-done(((bf16[704,512]{1,0:T(8,128)(2,1)}), bf16[704,2048]{1,0:T(8,128)(2,1)}) %all-gather.14.cloned.1.call-update) | async-done | bytes 2883600 | tf_op jit(solution)/shard_map/all_gather | solution.py:129
  250.7 12.1 %convolution_convert_fusion = bf16[1024,2048]{1,0:T(8,128)(2,1)} fusion(bf16[704,2048]{1,0:T(8,128)(2,1)} %all-gather.14.cloned.1.call-done, f32[1024,704]{0,1:T(8,128)} %fusion.18, bf16[2048,704]{0,1:T(8,128)(2,1)} %all-gather.10.cloned.1.call-done, bf16[2048,2048]{1,0:T(8,128)(2,1)} %constant_dynamic-update-slice_fusion, s32[]{:T(128)S(6)} %select_n.48), kind=kOutput, calls=%fused_computation.21 | convolution fusion | flops 5912002560 | bytes 17039364 | tf_op jit(solution)/shard_map/dot_general | solution.py:132
  262.8 43.4 %reduce-scatter.2.cloned.1.call-done = bf16[256,2048]{1,0:T(8,128)(2,1)} async-done(((bf16[1024,2048]{1,0:T(8,128)(2,1)}), bf16[256,2048]{1,0:T(8,128)(2,1)}) %reduce-scatter.2.cloned.1.call-update) | async-done | bytes 1048592 | tf_op jit(solution)/shard_map/reduce_scatter | solution.py:131
  306.2 2.5 add_convert_fusion
  (70 shorter events, 8.6 us)
Async XLA Ops:
  6.5 5.8 %copy-start = (bf16[1024,256]{1,0:T(8,128)(2,1)S(1)}, bf16[1024,256]{1,0:T(8,128)(2,1)}, u32[]{:S(2)}) copy-start(bf16[1024,256]{1,0:T(8,128)(2,1)} %param.15) | copy-start | bytes 1572868
  6.5 36.6 %all-gather.6.cloned.1.call-start = ((), (), s32[]{:S(2)}) async-start(), calls=%async_computation.2 | async-start | bytes 1310720 | tf_op jit(solution)/shard_map/all_gather | solution.py:99
  9.0 5.5 %copy-start.3 = (bf16[1024,256]{1,0:T(8,128)(2,1)S(1)}, bf16[1024,256]{1,0:T(8,128)(2,1)}, u32[]{:S(2)}) copy-start(bf16[1024,256]{1,0:T(8,128)(2,1)} %param.13) | copy-start | bytes 1572868
  12.3 59.8 %all-gather.8.cloned.1.call-start = ((), (), s32[]{:S(2)}) async-start(), calls=%async_computation.3 | async-start | bytes 1310720 | tf_op jit(solution)/shard_map/all_gather | solution.py:100
  13.1 189.8 %all-gather.12.cloned.1.call-start = ((), (), s32[]{:S(2)}) async-start(), calls=%async_computation.5 | async-start | bytes 3604480 | tf_op jit(solution)/shard_map/all_gather | solution.py:125
  13.8 196.8 %all-gather.10.cloned.1.call-start = ((), (), s32[]{:S(2)}) async-start(), calls=%async_computation.4 | async-start | bytes 3604480 | tf_op jit(solution)/shard_map/all_gather | solution.py:124
  14.4 236.3 %all-gather.14.cloned.1.call-start = ((), (), s32[]{:S(2)}) async-start(), calls=%async_computation.6 | async-start | bytes 3604480 | tf_op jit(solution)/shard_map/all_gather | solution.py:129
  15.5 7.2 %copy-start.5 = (f32[128]{0:T(128)S(1)}, f32[128]{0:T(128)}, u32[]{:S(2)}) copy-start(f32[128]{0:T(128)} %param.16) | copy-start | bytes 1540
  76.6 6.5 %copy-start.2 = (f32[1024,2048]{1,0:T(8,128)S(1)}, f32[1024,2048]{1,0:T(8,128)}, u32[]{:S(2)}) copy-start(f32[1024,2048]{1,0:T(8,128)} %get-tuple-element.174) | copy-start | bytes 25165828 | tf_op jit(solution)/shard_map/while
  90.5 5.9 %copy-start.2 = (f32[1024,2048]{1,0:T(8,128)S(1)}, f32[1024,2048]{1,0:T(8,128)}, u32[]{:S(2)}) copy-start(f32[1024,2048]{1,0:T(8,128)} %get-tuple-element.174) | copy-start | bytes 25165828 | tf_op jit(solution)/shard_map/while
  103.7 5.8 %copy-start.2 = (f32[1024,2048]{1,0:T(8,128)S(1)}, f32[1024,2048]{1,0:T(8,128)}, u32[]{:S(2)}) copy-start(f32[1024,2048]{1,0:T(8,128)} %get-tuple-element.174) | copy-start | bytes 25165828 | tf_op jit(solution)/shard_map/while
  117.0 5.8 %copy-start.2 = (f32[1024,2048]{1,0:T(8,128)S(1)}, f32[1024,2048]{1,0:T(8,128)}, u32[]{:S(2)}) copy-start(f32[1024,2048]{1,0:T(8,128)} %get-tuple-element.174) | copy-start | bytes 25165828 | tf_op jit(solution)/shard_map/while
  138.4 4.3 %copy-start.4 = (f32[2048]{0:T(1024)S(1)}, f32[2048]{0:T(1024)}, u32[]{:S(2)}) copy-start(f32[2048]{0:T(1024)} %param.20) | copy-start | bytes 24580
  142.9 14.4 %collective-permute-start = (bf16[256,2048]{1,0:T(8,128)(2,1)S(1)}, bf16[256,2048]{1,0:T(8,128)(2,1)}, u32[]{:S(2)}, u32[]{:S(2)}) collective-permute-start(bf16[256,2048]{1,0:T(8,128)(2,1)S(1)} %multiply_convert_fusion.1), channel_id=1, source_target_pairs={{0,1},{1,2},{2,3},{3,0},{4,5},{5,6},{6,7},{7,4},{8,9},{9,10},{10,1... | collective-permute-start | bytes 3145736 | tf_op jit(solution)/shard_map/ppermute | solution.py:17
  157.3 14.5 %collective-permute-start.1 = (bf16[256,2048]{1,0:T(8,128)(2,1)}, bf16[256,2048]{1,0:T(8,128)(2,1)}, u32[]{:S(2)}, u32[]{:S(2)}) collective-permute-start(bf16[256,2048]{1,0:T(8,128)(2,1)} %collective-permute-done), channel_id=1, source_target_pairs={{0,1},{1,2},{2,3},{3,0},{4,5},{5,6},{6,7},{7,4},{8,9},{9,10},{10,1... | collective-permute-start | bytes 3145736 | tf_op jit(solution)/shard_map/ppermute | solution.py:17
  157.3 149.0 %reduce-scatter.2.cloned.1.call-start = ((), (), s32[]{:S(2)}) async-start(), calls=%async_computation.7 | async-start | bytes 5242880 | tf_op jit(solution)/shard_map/reduce_scatter | solution.py:131
  171.8 14.5 %collective-permute-start.2 = (bf16[256,2048]{1,0:T(8,128)(2,1)}, bf16[256,2048]{1,0:T(8,128)(2,1)}, u32[]{:S(2)}, u32[]{:S(2)}) collective-permute-start(bf16[256,2048]{1,0:T(8,128)(2,1)} %collective-permute-done.1), channel_id=1, source_target_pairs={{0,1},{1,2},{2,3},{3,0},{4,5},{5,6},{6,7},{7,4},{8,9},{9,10},{10,1... | collective-permute-start | bytes 3145736 | tf_op jit(solution)/shard_map/ppermute | solution.py:17
  262.8 45.9 %copy-start.1 = (bf16[1024,256]{1,0:T(8,128)(2,1)S(1)}, bf16[1024,256]{1,0:T(8,128)(2,1)}, u32[]{:S(2)}) copy-start(bf16[1024,256]{1,0:T(8,128)(2,1)} %param.15) | copy-start | bytes 1572868
Sparse Core Ops, SparseCore 0:
  12.4 30.6 all-gather.5
  44.7 27.3 all-gather.7
  73.7 58.4 all-gather.11
  133.6 57.7 all-gather.9
  192.9 57.7 all-gather.13
  263.0 43.2 reduce-scatter.1
